TPU v7x, 32 devices: a whole 2x2x4 slice. The times are simulated.
32 devices in a mesh: grp: 2 (over x), ep: 16 (over z, y, core).
Axes of the slice: x: 2, y: 2, z: 4, core: 2. Of those that a mesh axis runs over, the one named last changes fastest.
Arguments:
- tokens: bfloat16 [32, 2048], P(('grp', 'ep')), parts along dimension 0, may hold values from -6 to 6
- cache_latent: bfloat16 [32, 3072, 512], P(('grp', 'ep')), parts along dimension 0, may hold values from -6 to 6
- cache_rope: bfloat16 [32, 32, 3072], P(('grp', 'ep')), parts along dimension 0, may hold values from -1000 to 1000
- lengths: int32 [32], P(('grp', 'ep')), parts along dimension 0, may hold values from 384 to 3072, as said below
- w_query: bfloat16 [2048, 1536], P('ep'), may hold values from -0.125 to 0.125
- w_latent: bfloat16 [2048, 512], P('ep'), may hold values from -0.125 to 0.125
- w_rope: bfloat16 [2048, 32], P('ep'), may hold values from -0.125 to 0.125
- w_absorb: bfloat16 [512, 1024], replicated, may hold values from -0.25 to 0.25
- w_value: bfloat16 [512, 1024], replicated, may hold values from -0.25 to 0.25
- w_output: bfloat16 [1024, 2048], P('ep'), may hold values from -0.1875 to 0.1875
- gain_attn: float32 [2048], replicated, may hold values from 0.1 to 1.9
- gain_latent: float32 [512], replicated, may hold values from 0.1 to 1.9
- gain_moe: float32 [2048], replicated, may hold values from 0.1 to 1.9
- routes: int32 [32, 2], P(('grp', 'ep')), parts along dimension 0, may hold values from 0 to 15, all different within a row; in each aligned block of 16 rows (0 to 15, 16 to 31, ...) at most 4 rows name the same one
- route_scores: float32 [32, 2], P(('grp', 'ep')), parts along dimension 0, may hold values from 0.2 to 1
- w_gate: bfloat16 [16, 2048, 512], P('ep'), may hold values from -0.125 to 0.125
- w_up: bfloat16 [16, 2048, 512], P('ep'), may hold values from -0.125 to 0.125
- w_down: bfloat16 [16, 512, 2048], P('ep'), may hold values from -0.25 to 0.25
Outputs:
- mixed: bfloat16 [32, 2048], P(('grp', 'ep')), parts along dimension 0
- new_latent: bfloat16 [32, 512], P(('grp', 'ep')), parts along dimension 0
- new_rope: bfloat16 [32, 32], P(('grp', 'ep')), parts along dimension 0
There are 2 independent parts, one for each index of `grp`. A program takes and returns all parts, laid end to end along the dimension named above; an argument that names none is the same for every part. Nothing has to cross between parts.
Inputs may be any that keep to these rules, and one draw needn't show every extreme that they name: `routes`: each row names 2 different experts; over one part's 16 tokens no expert is named by more than 4 rows, a bound that some block reaches. `lengths`: some sequence has all 3072 positions filled.
All inputs are finite; a program needn't handle non-finite values.
Results may differ from a plain program's by a relative error of at most 0.013.
Values may be sent and summed in bfloat16 or wider, within the bound.
A program may use at most 64 MiB of HBM per device.

v0:
```python
import jax
import jax.numpy as jnp
from jax import lax
from jax.sharding import PartitionSpec as P

D = 2048
HEADS = 16
NOPE = 64
ROPE = 32
VDIM = 64
LATENT = 512
CAP = 4


EPS = 1e-06
THETA = 10000.0


def rms_scale(values, gain):
    return values * lax.rsqrt(jnp.mean(values * values, axis=-1, keepdims=True) + EPS) * gain


def rope_tables(positions, width):
    inverse = THETA ** (-jnp.arange(0, width, 2).astype(jnp.float32) / width)
    angle = positions.astype(jnp.float32)[:, None] * inverse[None, :]
    return (jnp.cos(angle), jnp.sin(angle))


def apply_rope(values, cosine, sine):
    half = values.shape[-1] // 2
    first, second = (values[..., :half], values[..., half:])
    return jnp.concatenate(
        [first * cosine - second * sine, second * cosine + first * sine], axis=-1
    )


def body(
    tokens,
    cache_latent,
    cache_rope,
    lengths,
    w_query,
    w_latent,
    w_rope,
    w_absorb,
    w_value,
    w_output,
    gain_attn,
    gain_latent,
    gain_moe,
    routes,
    route_scores,
    w_gate,
    w_up,
    w_down,
):
    local_seqs = tokens.shape[0]
    devices = lax.axis_size("ep")
    q_width = w_query.shape[1]
    lat_width = w_latent.shape[1]
    normed = rms_scale(tokens.astype(jnp.float32), gain_attn).astype(jnp.bfloat16)
    feature_rows = lax.all_to_all(normed, "ep", split_axis=1, concat_axis=0, tiled=True)
    stacked = jnp.concatenate([w_query, w_latent, w_rope], axis=1)
    rows = feature_rows
    summed = lax.psum_scatter(
        jnp.dot(rows, stacked, preferred_element_type=jnp.float32),
        "ep",
        scatter_dimension=0,
        tiled=True,
    )
    query = summed[:, :q_width].astype(jnp.bfloat16)
    latent_raw = summed[:, q_width : q_width + lat_width].astype(jnp.bfloat16)
    rope_raw = summed[:, q_width + lat_width :].astype(jnp.bfloat16)
    new_latent = rms_scale(latent_raw.astype(jnp.float32), gain_latent).astype(jnp.bfloat16)
    cosine, sine = rope_tables(lengths, ROPE)
    new_rope = apply_rope(rope_raw.astype(jnp.float32), cosine, sine).astype(jnp.bfloat16)
    heads_view = query.reshape(local_seqs, HEADS, NOPE + ROPE)
    q_nope = heads_view[:, :, :NOPE]
    q_pe = apply_rope(
        heads_view[:, :, NOPE:].astype(jnp.float32), cosine[:, None, :], sine[:, None, :]
    ).astype(jnp.bfloat16)
    q_abs = jnp.einsum(
        "shn,chn->shc",
        q_nope,
        w_absorb.reshape(LATENT, HEADS, NOPE),
        preferred_element_type=jnp.float32,
    ).astype(jnp.bfloat16)
    scale = (NOPE + ROPE) ** (-0.5)
    past = (
        jnp.einsum("shc,skc->shk", q_abs, cache_latent, preferred_element_type=jnp.float32)
        + jnp.einsum("shr,srk->shk", q_pe, cache_rope, preferred_element_type=jnp.float32)
    ) * scale
    fresh = (
        jnp.einsum("shc,sc->sh", q_abs, new_latent, preferred_element_type=jnp.float32)
        + jnp.einsum("shr,sr->sh", q_pe, new_rope, preferred_element_type=jnp.float32)
    ) * scale
    valid = jnp.arange(cache_latent.shape[1])[None, None, :] < lengths[:, None, None]
    top = jnp.maximum(jnp.max(jnp.where(valid, past, -jnp.inf), axis=-1), fresh)
    e_past = jnp.where(valid, jnp.exp(past - top[:, :, None]), 0.0)
    e_new = jnp.exp(fresh - top)
    total = jnp.sum(e_past, axis=-1) + e_new
    p_past = (e_past / total[:, :, None]).astype(jnp.bfloat16)
    p_new = (e_new / total).astype(jnp.bfloat16)
    attended = (
        jnp.einsum("shk,skc->shc", p_past, cache_latent, preferred_element_type=jnp.float32)
        + p_new.astype(jnp.float32)[:, :, None] * new_latent.astype(jnp.float32)[:, None, :]
    ).astype(jnp.bfloat16)
    values = jnp.einsum(
        "shc,chv->shv",
        attended,
        w_value.reshape(LATENT, HEADS, VDIM),
        preferred_element_type=jnp.float32,
    ).astype(jnp.bfloat16)
    values = values.reshape(local_seqs, HEADS * VDIM)
    head_rows = lax.all_to_all(values, "ep", split_axis=1, concat_axis=0, tiled=True)
    rows = head_rows
    attn_out = lax.psum_scatter(
        jnp.dot(rows, w_output, preferred_element_type=jnp.float32),
        "ep",
        scatter_dimension=0,
        tiled=True,
    )
    resid = (tokens.astype(jnp.float32) + attn_out).astype(jnp.bfloat16)
    moe_in = rms_scale(resid.astype(jnp.float32), gain_moe).astype(jnp.bfloat16)
    route_weight = route_scores / jnp.sum(route_scores, axis=-1, keepdims=True)
    slots = jnp.arange(CAP).astype(jnp.float32)
    expert_ids = jnp.arange(devices)
    hits = routes[:, :, None] == expert_ids[None, None, :]
    chosen = jnp.any(hits, axis=1)
    outgoing = jnp.where(chosen.T[:, :, None], moe_in[None, :, :], jnp.zeros((), jnp.bfloat16))
    flags_out = chosen.T.astype(jnp.bfloat16)
    arrived, arrived_flags = (
        lax.all_to_all(outgoing, "ep", split_axis=0, concat_axis=0, tiled=True),
        lax.all_to_all(flags_out, "ep", split_axis=0, concat_axis=0, tiled=True),
    )
    flat_rows = arrived.reshape(devices * local_seqs, D)
    flag = arrived_flags.reshape(-1).astype(jnp.float32)
    rank = jnp.cumsum(flag) - 1.0
    picker = ((rank[None, :] == slots[:, None]) & (flag[None, :] > 0.5)).astype(jnp.bfloat16)
    packed = jnp.dot(picker, flat_rows, preferred_element_type=jnp.float32).astype(jnp.bfloat16)
    gate = jnp.dot(packed, w_gate[0], preferred_element_type=jnp.float32)
    upper = jnp.dot(packed, w_up[0], preferred_element_type=jnp.float32)
    hidden = (jax.nn.silu(gate) * upper).astype(jnp.bfloat16)
    result = jnp.dot(hidden, w_down[0], preferred_element_type=jnp.float32).astype(jnp.bfloat16)
    spread = (
        jnp.dot(picker.T, result, preferred_element_type=jnp.float32)
        .astype(jnp.bfloat16)
        .reshape(devices, local_seqs, D)
    )
    answers = lax.all_to_all(spread, "ep", split_axis=0, concat_axis=0, tiled=True)
    weight_table = jnp.sum(hits.astype(jnp.float32) * route_weight[:, :, None], axis=1)
    moe_sum = jnp.einsum("sn,nsd->sd", weight_table, answers.astype(jnp.float32))
    mixed = (resid.astype(jnp.float32) + moe_sum).astype(jnp.bfloat16)
    return (mixed, new_latent, new_rope)


def solution(mesh):
    placed = (
        P(("grp", "ep"), None),
        P(("grp", "ep"), None, None),
        P(("grp", "ep"), None, None),
        P(("grp", "ep")),
        P("ep", None),
        P("ep", None),
        P("ep", None),
        P(),
        P(),
        P("ep", None),
        P(),
        P(),
        P(),
        P(("grp", "ep"), None),
        P(("grp", "ep"), None),
        P("ep", None, None),
        P("ep", None, None),
        P("ep", None, None),
    )
    return jax.shard_map(
        body,
        mesh=mesh,
        in_specs=placed,
        out_specs=(P(("grp", "ep"), None), P(("grp", "ep"), None), P(("grp", "ep"), None)),
        check_vma=False,
    )
```

profile of v0, /device:TPU:0, one launch (start us, length us, event | category | flops | bytes accessed | tf_op | source)
XLA Modules:
  0.0 251.2 jit_solution(14242424086697697236)
XLA Ops:
  7.2 1.5 multiply_reduce_fusion.1
  9.3 1.3 convert_bitcast_fusion
  10.7 7.4 %all-to-all-start = ((bf16[1,16,128]{2,0,1:T(2,128)(2,1)}), bf16[1,16,128]{2,0,1:T(2,128)(2,1)S(1)}, u32[]{:S(2)}, u32[]{:S(2)}) async-start(bf16[1,16,128]{2,0,1:T(2,128)(2,1)} %convert_bitcast_fusion), calls=%async_computation | async-start | bytes 16384 | tf_op jit(solution)/shard_map/all_to_all | solution.py:62
  18.8 0.7 fusion.67
  20.6 0.8 copy.40
  21.5 2.3 copy.41
  23.8 2.3 copy.42
  26.7 0.7 reduce_sum.57
  27.3 1.3 fusion.30
  28.6 63.5 %all-reduce.6 = bf16[16,2080]{1,0:T(8,128)(2,1)S(1)} all-reduce(f32[16,2080]{1,0:T(8,128)S(1)} %fusion.30), channel_id=2, replica_groups=mesh['grp'=2,'ep'=16] {'ep'}, use_global_device_ids=true, to_apply=%region_1.0.clone | all-reduce | flops 33280 | bytes 199680
  92.1 0.7 dynamic-slice_convert_fusion
  94.4 0.7 fusion.86
  95.1 1.5 fusion.51
  96.7 0.7 fusion.56
  97.6 1.0 select_reduce_fusion
  100.9 3.5 %all-to-all-start.1 = ((bf16[1,16,64]{2,0,1:T(2,128)(2,1)}), bf16[1,16,64]{2,0,1:T(2,128)(2,1)S(1)}, u32[]{:S(2)}, u32[]{:S(2)}) async-start(bf16[1,16,64]{2,0,1:T(2,128)(2,1)} %copy.43), calls=%async_computation.1 | async-start | bytes 16384 | tf_op jit(solution)/shard_map/all_to_all | solution.py:115
  105.0 0.7 copy.44
  105.7 5.0 %all-to-all-done.1 = bf16[1,16,64]{2,0,1:T(2,128)(2,1)S(1)} async-done(((bf16[1,16,64]{2,0,1:T(2,128)(2,1)}), bf16[1,16,64]{2,0,1:T(2,128)(2,1)S(1)}, u32[]{:S(2)}, u32[]{:S(2)}) %all-to-all-start.1) | async-done | bytes 2080 | tf_op jit(solution)/shard_map/all_to_all | solution.py:115
  110.7 3.5 %all-to-all-start.2 = ((bf16[16,1,1]{2,1,0:T(2,128)(2,1)}), bf16[16,1,1]{2,1,0:T(2,128)(2,1)S(1)}, u32[]{:S(2)}, u32[]{:S(2)}) async-start(bf16[16,1,1]{2,1,0:T(2,128)(2,1)} %copy.44), calls=%async_computation.2 | async-start | bytes 16384 | tf_op jit(solution)/shard_map/all_to_all | solution.py:134
  114.3 0.8 fusion.58
  115.1 5.5 %all-to-all-done.2 = bf16[16,1,1]{2,1,0:T(2,128)(2,1)S(1)} async-done(((bf16[16,1,1]{2,1,0:T(2,128)(2,1)}), bf16[16,1,1]{2,1,0:T(2,128)(2,1)S(1)}, u32[]{:S(2)}, u32[]{:S(2)}) %all-to-all-start.2) | async-done | bytes 64 | tf_op jit(solution)/shard_map/all_to_all | solution.py:134
  120.6 87.4 %all-reduce.5.cloned.1.call-done = f32[16,2048]{1,0:T(8,128)} async-done(((f32[16,2048]{1,0:T(8,128)}), f32[16,2048]{1,0:T(8,128)}) %all-reduce.5.cloned.1.call-update) | async-done | bytes 131088
  208.0 2.1 multiply_reduce_fusion
  211.6 1.0 reduce.20
  213.2 6.3 %all-to-all-start.3 = ((bf16[16,2,1024]{2,1,0:T(2,128)(2,1)}), bf16[16,2,1024]{2,1,0:T(2,128)(2,1)S(1)}, u32[]{:S(2)}, u32[]{:S(2)}) async-start(bf16[16,2,1024]{2,1,0:T(2,128)(2,1)} %reshape.512), calls=%async_computation.3 | async-start | bytes 131072 | tf_op jit(solution)/shard_map/all_to_all | solution.py:133
  220.0 6.4 %all-to-all-done.3 = bf16[16,2,1024]{2,1,0:T(2,128)(2,1)S(1)} async-done(((bf16[16,2,1024]{2,1,0:T(2,128)(2,1)}), bf16[16,2,1024]{2,1,0:T(2,128)(2,1)S(1)}, u32[]{:S(2)}, u32[]{:S(2)}) %all-to-all-start.3) | async-done | bytes 65568 | tf_op jit(solution)/shard_map/all_to_all | solution.py:133
  226.7 2.0 fusion.9
  228.6 3.0 %convolution_convert_fusion.1 = bf16[4,2048]{1,0:T(4,128)(2,1)S(1)} fusion(bf16[1,512,2048]{2,1,0:T(8,128)(2,1)} %param.35, bf16[4,2048]{1,0:T(4,128)(2,1)S(1)} %convolution_convert_fusion.2, bf16[1,2048,512]{2,1,0:T(8,128)(2,1)} %param.34, f32[4,512]{1,0:T(4,128)S(1)} %fusion.9), kind=kOutput, calls=%fused_computation.7 | convolution fusion | flops 16797696 | bytes 4235264 | tf_op jit(solution)/shard_map/dot_general | solution.py:144
  231.9 0.7 reduce.21
  233.2 3.5 %all-to-all-start.4 = ((bf16[16,2,1024]{2,1,0:T(2,128)(2,1)}), bf16[16,2,1024]{2,1,0:T(2,128)(2,1)S(1)}, u32[]{:S(2)}, u32[]{:S(2)}) async-start(bf16[16,2,1024]{2,1,0:T(2,128)(2,1)} %reshape.514), calls=%async_computation.4 | async-start | bytes 131072 | tf_op jit(solution)/shard_map/all_to_all | solution.py:150
  237.4 6.2 %all-to-all-done.4 = bf16[16,2,1024]{2,1,0:T(2,128)(2,1)S(1)} async-done(((bf16[16,2,1024]{2,1,0:T(2,128)(2,1)}), bf16[16,2,1024]{2,1,0:T(2,128)(2,1)S(1)}, u32[]{:S(2)}, u32[]{:S(2)}) %all-to-all-start.4) | async-done | bytes 65568 | tf_op jit(solution)/shard_map/all_to_all | solution.py:150
  243.6 0.8 fusion.5
  (69 shorter events, 9.6 us)
Async XLA Ops:
  7.2 90.5 %copy-start = (bf16[1,3072,512]{2,1,0:T(8,128)(2,1)S(1)}, bf16[1,3072,512]{2,1,0:T(8,128)(2,1)}, u32[]{:S(2)}) copy-start(bf16[1,3072,512]{2,1,0:T(8,128)(2,1)} %param.19) | copy-start | bytes 9437188
  10.7 16.7 %all-to-all-start = ((bf16[1,16,128]{2,0,1:T(2,128)(2,1)}), bf16[1,16,128]{2,0,1:T(2,128)(2,1)S(1)}, u32[]{:S(2)}, u32[]{:S(2)}) async-start(bf16[1,16,128]{2,0,1:T(2,128)(2,1)} %convert_bitcast_fusion), calls=%async_computation | async-start | bytes 16384 | tf_op jit(solution)/shard_map/all_to_all | solution.py:62
  19.5 6.6 %copy-start.7 = (pred[16]{0:T(512)(128)(4,1)}, pred[16]{0:T(512)(128)(4,1)S(1)}, u32[]{:S(2)}) copy-start(pred[16]{0:T(512)(128)(4,1)S(1)} %fusion.67) | copy-start | bytes 52
  21.4 4.7 %copy-start.13 = (u32[32]{0:T(128)S(1)}, u32[32]{0:T(128)}, u32[]{:S(2)}) copy-start(u32[32]{0:T(128)} %constant.56) | copy-start | bytes 388
  21.4 5.2 %copy-start.10 = (f32[1,2]{1,0:T(1,128)S(1)}, f32[1,2]{1,0:T(1,128)}, u32[]{:S(2)}) copy-start(f32[1,2]{1,0:T(1,128)} %param.32) | copy-start | bytes 28
  23.8 73.6 %copy-start.3 = (bf16[1,32,3072]{2,1,0:T(8,128)(2,1)S(1)}, bf16[1,32,3072]{2,1,0:T(8,128)(2,1)}, u32[]{:S(2)}) copy-start(bf16[1,32,3072]{2,1,0:T(8,128)(2,1)} %param.20) | copy-start | bytes 589828
  95.1 3.6 %copy-start.6 = (bf16[1,512]{1,0:T(2,128)(2,1)}, bf16[1,512]{1,0:T(2,128)(2,1)S(1)}, u32[]{:S(2)}) copy-start(bf16[1,512]{1,0:T(2,128)(2,1)S(1)} %get-tuple-element.6) | copy-start | bytes 3076
  98.7 1.2 copy-start.1
  99.1 5.3 %copy-start.11 = (f32[1,2]{1,0:T(1,128)S(1)}, f32[1,2]{1,0:T(1,128)}, u32[]{:S(2)}) copy-start(f32[1,2]{1,0:T(1,128)} %param.32) | copy-start | bytes 28
  99.1 5.9 %copy-start.9 = (bf16[16,1,1]{0,2,1:T(2,128)(2,1)S(1)}, bf16[16,1,1]{0,2,1:T(2,128)(2,1)}, u32[]{:S(2)}) copy-start(bf16[16,1,1]{0,2,1:T(2,128)(2,1)} %convert_bitcast_fusion.2) | copy-start | bytes 100
  99.1 15.1 %copy-start.2 = (bf16[64,2048]{1,0:T(8,128)(2,1)S(1)}, bf16[64,2048]{1,0:T(8,128)(2,1)}, u32[]{:S(2)}) copy-start(bf16[64,2048]{1,0:T(8,128)(2,1)} %param.27) | copy-start | bytes 786436
  99.2 108.9 %copy-start.4 = (bf16[1,2048]{1,0:T(2,128)(2,1)S(1)}, bf16[1,2048]{1,0:T(2,128)(2,1)}, u32[]{:S(2)}) copy-start(bf16[1,2048]{1,0:T(2,128)(2,1)} %param.18) | copy-start | bytes 12292
  99.2 111.7 %copy-start.5 = (f32[2048]{0:T(1024)S(1)}, f32[2048]{0:T(1024)}, u32[]{:S(2)}) copy-start(f32[2048]{0:T(1024)} %param.30) | copy-start | bytes 24580
  99.2 111.7 %copy-start.8 = (pred[16]{0:T(512)(128)(4,1)S(1)}, pred[16]{0:T(512)(128)(4,1)}, u32[]{:S(2)}) copy-start(pred[16]{0:T(512)(128)(4,1)} %copy-done.7) | copy-start | bytes 52
  100.9 9.8 %all-to-all-start.1 = ((bf16[1,16,64]{2,0,1:T(2,128)(2,1)}), bf16[1,16,64]{2,0,1:T(2,128)(2,1)S(1)}, u32[]{:S(2)}, u32[]{:S(2)}) async-start(bf16[1,16,64]{2,0,1:T(2,128)(2,1)} %copy.43), calls=%async_computation.1 | async-start | bytes 16384 | tf_op jit(solution)/shard_map/all_to_all | solution.py:115
  110.7 9.9 %all-to-all-start.2 = ((bf16[16,1,1]{2,1,0:T(2,128)(2,1)}), bf16[16,1,1]{2,1,0:T(2,128)(2,1)S(1)}, u32[]{:S(2)}, u32[]{:S(2)}) async-start(bf16[16,1,1]{2,1,0:T(2,128)(2,1)} %copy.44), calls=%async_computation.2 | async-start | bytes 16384 | tf_op jit(solution)/shard_map/all_to_all | solution.py:134
  114.2 93.8 %all-reduce.5.cloned.1.call-start = ((), (), s32[]{:S(2)}) async-start(), calls=%async_computation.5 | async-start | bytes 262144
  213.2 13.2 %all-to-all-start.3 = ((bf16[16,2,1024]{2,1,0:T(2,128)(2,1)}), bf16[16,2,1024]{2,1,0:T(2,128)(2,1)S(1)}, u32[]{:S(2)}, u32[]{:S(2)}) async-start(bf16[16,2,1024]{2,1,0:T(2,128)(2,1)} %reshape.512), calls=%async_computation.3 | async-start | bytes 131072 | tf_op jit(solution)/shard_map/all_to_all | solution.py:133
  228.6 8.1 %copy-start.12 = (s32[1,2]{1,0:T(1,128)S(1)}, s32[1,2]{1,0:T(1,128)}, u32[]{:S(2)}) copy-start(s32[1,2]{1,0:T(1,128)} %param.31) | copy-start | bytes 28
  233.2 10.4 %all-to-all-start.4 = ((bf16[16,2,1024]{2,1,0:T(2,128)(2,1)}), bf16[16,2,1024]{2,1,0:T(2,128)(2,1)S(1)}, u32[]{:S(2)}, u32[]{:S(2)}) async-start(bf16[16,2,1024]{2,1,0:T(2,128)(2,1)} %reshape.514), calls=%async_computation.4 | async-start | bytes 131072 | tf_op jit(solution)/shard_map/all_to_all | solution.py:150
Sparse Core Ops, SparseCore 0:
  118.5 89.5 all-reduce.4
where the time goes:
time: 252 us; the launch traced here: 251 us
  waiting for transfers between devices  110 us (44%)
  blocking collectives  63.5 us (25%)
  starting transfers between devices  24.2 us (10%)
  between operations  17.1 us (7%)
  other arithmetic  13.6 us (5%)
  matrix products  12.2 us (5%)
  local copies, waits for them, and re-layouts  10.3 us (4%)
    unnamed x2, waiting for transfers between devices  87.4 us
    unnamed x1, blocking collectives  63.5 us
    unnamed x36, local copies, waits for them, and re-layouts  7.66 us
    all_to_all x1, starting transfers between devices, body(): lax.all_to_all(normed, 'ep', split_axis=1, concat_axis=0, tiled=True)  7.41 us
    all_to_all x1, waiting for transfers between devices, body(): lax.all_to_all(outgoing, 'ep', split_axis=0, concat_axis=0, tiled=True)  6.39 us
    all_to_all x1, starting transfers between devices, body(): lax.all_to_all(outgoing, 'ep', split_axis=0, concat_axis=0, tiled=True)  6.26 us
    all_to_all x1, waiting for transfers between devices, body(): lax.all_to_all(spread, 'ep', split_axis=0, concat_axis=0, tiled=True)  6.17 us
    all_to_all x1, waiting for transfers between devices, body(): lax.all_to_all(flags_out, 'ep', split_axis=0, concat_axis=0, tiled=True)  5.49 us
  transfers between devices with their start and end apart: 6, of which 5 were waited for; matrix products, arithmetic and copies ran while one was open for 5% of the time, Pallas kernels for 0%

commit v1 on v0

v1 whole, which is shorter than its diff:
```python
import functools
import jax
import jax.numpy as jnp
from jax import lax
from jax.experimental import pallas as pl
from jax.experimental.pallas import tpu as pltpu
from jax.sharding import PartitionSpec as P

HEADS = 16
NOPE = 64
ROPE = 32
VDIM = 64
EPS = 1e-06
THETA = 10000.0
LANES = 128
F32 = jnp.float32
BF16 = jnp.bfloat16
MESH = pl.DeviceIdType.MESH


def dot(a, b):
    return jnp.dot(a, b, preferred_element_type=F32)


def dot_t(a, b):
    return lax.dot_general(a, b, (((1,), (1,)), ((), ())), preferred_element_type=F32)


def rms_scale(values, gain):
    return values * lax.rsqrt(jnp.mean(values * values, axis=-1, keepdims=True) + EPS) * gain


def iota(shape, dim):
    return lax.broadcasted_iota(jnp.int32, shape, dim)


def ones_where(mask):
    return jnp.where(mask, 1.0, 0.0).astype(BF16)


def kernel(
    n,
    tok_ref, table_ref, g_attn_ref, g_lat_ref, g_moe_ref, len_ref, route_ref, score_ref,
    cache_hbm, crope_hbm, wq_hbm, wl_hbm, wr_hbm, wa_hbm, wv_hbm, wo_hbm, wg_hbm, wu_hbm, wd_hbm,
    mixed_ref, nlat_ref, nrope_ref,
    cache, crope, wq, wl, wr, wa, wv, wo, wg, wu, wd,
    send1, recv1, rows1, send2, recv2, send3, recv3, rows3, send4, recv4, send5, recv5, rows5,
    send6, recv6, local_sem, link_sem,
):
    me = lax.axis_index("ep")
    pairs = [
        (wq_hbm, wq), (wl_hbm, wl), (wr_hbm, wr), (wa_hbm, wa), (crope_hbm.at[0], crope),
        (cache_hbm.at[0], cache), (wv_hbm, wv), (wo_hbm, wo),
        (wg_hbm.at[0], wg), (wu_hbm.at[0], wu), (wd_hbm.at[0], wd),
    ]
    loads = [pltpu.make_async_copy(a, b, local_sem.at[i]) for i, (a, b) in enumerate(pairs)]
    for load in loads:
        load.start()
    (l_wq, l_wl, l_wr, l_wa, l_crope, l_cache, l_wv, l_wo, l_wg, l_wu, l_wd) = loads

    barrier = pltpu.get_barrier_semaphore()

    def greet(k, carry):
        pl.semaphore_signal(
            barrier, inc=1, device_id={"ep": lax.rem(me + k, n)}, device_id_type=MESH
        )
        return carry

    lax.fori_loop(1, n, greet, 0)

    def copy(phase, source, target, peer, slot):
        return pltpu.make_async_remote_copy(
            src_ref=source(peer),
            dst_ref=target.at[slot],
            send_sem=link_sem.at[phase, 0, peer],
            recv_sem=link_sem.at[phase, 1, slot],
            device_id={"ep": peer},
            device_id_type=MESH,
        )

    def send(phase, source, target):
        def step(k, carry):
            copy(phase, source, target, lax.rem(me + k, n), me).start()
            return carry

        lax.fori_loop(1, n, step, 0)

    def receive(phase, source, target):
        def step(k, carry):
            peer = lax.rem(me + n - k, n)
            copy(phase, source, target, peer, peer).wait_recv()
            return carry

        lax.fori_loop(1, n, step, 0)

    def sent(phase, source, target):
        def step(k, carry):
            peer = lax.rem(me + k, n)
            copy(phase, source, target, peer, peer).wait_send()
            return carry

        lax.fori_loop(1, n, step, 0)

    def gather_rows(buffer, rows):
        for t in range(n):
            rows[t : t + 1, :] = buffer[t]

    tokens = tok_ref[...].astype(F32)
    normed = rms_scale(tokens, g_attn_ref[...]).astype(BF16).astype(F32)
    depth = wq.shape[0]
    for t in range(n):
        send1[t] = normed[:, t * depth : (t + 1) * depth]
    recv1[me] = send1[me]
    pl.semaphore_wait(barrier, n - 1)
    src1 = lambda peer: send1.at[peer]
    send(0, src1, recv1)
    qw, lw, rw = wq.shape[1], wl.shape[1], wr.shape[1]
    l_wq.wait()
    l_wl.wait()
    l_wr.wait()
    receive(0, src1, recv1)
    gather_rows(recv1, rows1)
    rows = rows1[...].astype(BF16)
    part_q = dot(rows, wq[...])
    part_l = dot(rows, wl[...])
    part_r = dot(rows, wr[...])
    for t in range(n):
        send2[t, :, :qw] = part_q[t : t + 1]
        send2[t, :, qw : qw + lw] = part_l[t : t + 1]
        send2[t, :, qw + lw : qw + lw + rw] = part_r[t : t + 1]
    recv2[me] = send2[me]
    src2 = lambda peer: send2.at[peer]
    send(1, src2, recv2)
    sel = jnp.concatenate([ones_where(iota((NOPE + ROPE, LANES), 0) == iota((NOPE + ROPE, LANES), 1))] * HEADS, axis=0)
    head_width = NOPE + ROPE
    own_q = iota((HEADS, qw), 1) - head_width * iota((HEADS, qw), 0)
    own_q = (own_q >= 0) & (own_q < head_width)
    spread = ones_where((iota((LANES, HEADS * NOPE), 1) & (NOPE - 1)) == iota((LANES, HEADS * NOPE), 0))
    own_n = iota((HEADS, HEADS * NOPE), 1) - NOPE * iota((HEADS, HEADS * NOPE), 0)
    own_n = (own_n >= 0) & (own_n < NOPE)
    half = ROPE // 2
    lane = iota((LANES, ROPE), 1)
    swapped = jnp.where(lane < half, lane + half, lane - half)
    pick = ones_where(iota((LANES, ROPE), 0) == NOPE + lane)
    pick_swap = ones_where(iota((LANES, ROPE), 0) == NOPE + swapped)
    swap = ones_where(iota((ROPE, ROPE), 0) == swapped[:ROPE])
    cosine, sine = table_ref[0:1, :], table_ref[1:2, :]
    receive(1, src2, recv2)
    summed = jnp.sum(recv2[:, :, : qw + lw + LANES], axis=0)
    latent_raw = summed[:, qw : qw + lw].astype(BF16).astype(F32)
    new_latent = rms_scale(latent_raw, g_lat_ref[...]).astype(BF16)
    nlat_ref[...] = new_latent
    new_latent = new_latent.astype(F32)
    rope_raw = jnp.broadcast_to(summed[:, qw + lw : qw + lw + rw].astype(BF16).astype(F32), (HEADS, rw))
    new_rope = rope_raw * cosine + dot(rope_raw.astype(BF16), swap) * sine
    new_rope = new_rope.astype(BF16)
    nrope_ref[...] = new_rope[0:1, :]
    new_rope = new_rope.astype(F32)
    query = jnp.broadcast_to(summed[:, :qw].astype(BF16).astype(F32), (HEADS, qw))
    query = jnp.where(own_q, query, 0.0).astype(BF16)
    heads = dot(query, sel).astype(BF16)
    q_pe = (dot(heads, pick) * cosine + dot(heads, pick_swap) * sine).astype(BF16)
    q_diag = jnp.where(own_n, dot(heads, spread), 0.0).astype(BF16)
    l_wa.wait()
    q_abs = dot_t(q_diag, wa[...]).astype(BF16)
    scale = (NOPE + ROPE) ** (-0.5)
    l_crope.wait()
    l_cache.wait()
    past = (dot_t(q_abs, cache[...]) + dot(q_pe, crope[...])) * scale
    fresh = (
        jnp.sum(q_abs.astype(F32) * new_latent, axis=-1, keepdims=True)
        + jnp.sum(q_pe.astype(F32) * new_rope, axis=-1, keepdims=True)
    ) * scale
    past = jnp.where(iota(past.shape, 1) < len_ref[0], past, -jnp.inf)
    top = jnp.maximum(jnp.max(past, axis=-1, keepdims=True), fresh)
    e_past = jnp.exp(past - top)
    e_new = jnp.exp(fresh - top)
    total = jnp.sum(e_past, axis=-1, keepdims=True) + e_new
    inverse = 1.0 / total
    p_past = (e_past * inverse).astype(BF16)
    p_new = (e_new * inverse).astype(BF16).astype(F32)
    attended = (dot(p_past, cache[...]) + p_new * new_latent).astype(BF16)
    l_wv.wait()
    values = dot(attended, wv[...])
    values = jnp.sum(jnp.where(own_n, values, 0.0), axis=0, keepdims=True).astype(BF16).astype(F32)
    for t in range(send3.shape[0]):
        send3[t] = values[:, t * LANES : (t + 1) * LANES]
    width = wo.shape[0]
    group = LANES // width
    recv3[me] = send3[me // group]
    src3 = lambda peer: send3.at[peer // group]
    send(2, src3, recv3)
    l_wo.wait()
    cut = ones_where(iota((LANES, width), 0) == iota((LANES, width), 1) + width * lax.rem(me, group))
    receive(2, src3, recv3)
    gather_rows(recv3, rows3)
    rows = dot(rows3[...].astype(BF16), cut).astype(BF16)
    part = dot(rows, wo[...])
    for t in range(n):
        send4[t] = part[t : t + 1]
    recv4[me] = send4[me]
    src4 = lambda peer: send4.at[peer]
    send(3, src4, recv4)
    receive(3, src4, recv4)
    resid = (tokens + jnp.sum(recv4[...], axis=0)).astype(BF16).astype(F32)
    moe_in = rms_scale(resid, g_moe_ref[...]).astype(BF16).astype(F32)
    send5[0] = moe_in
    recv5[me] = moe_in
    src5 = lambda peer: send5.at[0]
    send(4, src5, recv5)
    l_wg.wait()
    l_wu.wait()
    l_wd.wait()
    receive(4, src5, recv5)
    gather_rows(recv5, rows5)
    rows = rows5[...].astype(BF16)
    gate = dot(rows, wg[...])
    upper = dot(rows, wu[...])
    hidden = (jax.nn.silu(gate) * upper).astype(BF16)
    result = dot(hidden, wd[...]).astype(BF16).astype(F32)
    for t in range(n):
        send6[t] = result[t : t + 1]
    recv6[me] = send6[me]
    src6 = lambda peer: send6.at[peer]
    send(5, src6, recv6)
    topk = route_ref.shape[1]
    weight = score_ref[0, 0]
    for k in range(1, topk):
        weight = weight + score_ref[0, k]
    receive(5, src6, recv6)
    moe_sum = jnp.zeros_like(resid)
    for k in range(topk):
        moe_sum = moe_sum + (jnp.full(resid.shape, score_ref[0, k]) / weight) * recv6[route_ref[0, k]]
    mixed_ref[...] = (resid + moe_sum).astype(BF16)
    sent(0, src1, recv1)
    sent(1, src2, recv2)
    sent(2, src3, recv3)
    sent(3, src4, recv4)
    sent(4, src5, recv5)
    sent(5, src6, recv6)


def body(
    tokens, cache_latent, cache_rope, lengths, w_query, w_latent, w_rope, w_absorb, w_value,
    w_output, gain_attn, gain_latent, gain_moe, routes, route_scores, w_gate, w_up, w_down,
):
    n = lax.axis_size("ep")
    d = tokens.shape[1]
    total = w_query.shape[1] + w_latent.shape[1] + LANES
    inverse = THETA ** (-jnp.arange(0, ROPE, 2).astype(F32) / ROPE)
    angle = lengths.astype(F32)[:, None] * inverse[None, :]
    cosine, sine = jnp.cos(angle), jnp.sin(angle)
    table = jnp.concatenate(
        [jnp.concatenate([cosine, cosine], axis=1), jnp.concatenate([-sine, sine], axis=1)], axis=0
    )
    vmem = pl.BlockSpec(memory_space=pltpu.VMEM)
    smem = pl.BlockSpec(memory_space=pltpu.SMEM)
    hbm = pl.BlockSpec(memory_space=pl.ANY)

    def like(a):
        return pltpu.VMEM(a.shape[-2:], a.dtype)

    big = [w_query, w_latent, w_rope, w_absorb, w_value, w_output, w_gate, w_up, w_down]
    depth = w_query.shape[0]
    tiles = w_value.shape[1] // LANES
    row = lambda count, wide: pltpu.VMEM((count, 1, wide), F32)
    return pl.pallas_call(
        functools.partial(kernel, n),
        out_shape=(
            jax.ShapeDtypeStruct(tokens.shape, BF16),
            jax.ShapeDtypeStruct((1, w_latent.shape[1]), BF16),
            jax.ShapeDtypeStruct((1, w_rope.shape[1]), BF16),
        ),
        in_specs=[vmem] * 5 + [smem] * 3 + [hbm] * 11,
        out_specs=(vmem, vmem, vmem),
        scratch_shapes=[like(cache_latent), like(cache_rope)]
        + [like(a) for a in big]
        + [
            row(n, depth), row(n, depth), pltpu.VMEM((n, depth), F32),
            row(n, total), row(n, total),
            row(tiles, LANES), row(n, LANES), pltpu.VMEM((n, LANES), F32),
            row(n, d), row(n, d),
            row(1, d), row(n, d), pltpu.VMEM((n, d), F32),
            row(n, d), row(n, d),
            pltpu.SemaphoreType.DMA((11,)),
            pltpu.SemaphoreType.DMA((6, 2, n)),
        ],
        compiler_params=pltpu.CompilerParams(
            collective_id=0, has_side_effects=True, vmem_limit_bytes=56 * 1024 * 1024
        ),
    )(
        tokens, table, gain_attn[None, :], gain_latent[None, :], gain_moe[None, :], lengths, routes,
        route_scores, cache_latent, cache_rope, w_query, w_latent, w_rope, w_absorb, w_value,
        w_output, w_gate, w_up, w_down,
    )


def solution(mesh):
    rows = P(("grp", "ep"), None)
    cube = P(("grp", "ep"), None, None)
    split = P("ep", None)
    placed = (
        rows, cube, cube, P(("grp", "ep")), split, split, split, P(), P(), split, P(), P(), P(),
        rows, rows, P("ep", None, None), P("ep", None, None), P("ep", None, None),
    )
    return jax.shard_map(
        body, mesh=mesh, in_specs=placed, out_specs=(rows, rows, rows), check_vma=False
    )
```

time: 252 us -> 49 us (0.19)
  waiting for transfers between devices: 110 us -> 0 us
  blocking collectives: 63.5 us -> 0 us
  Pallas kernels: 0 us -> 41.5 us
  starting transfers between devices: 24.2 us -> 0 us
  between operations: 17.1 us -> 1.3 us
  other arithmetic: 13.6 us -> 0.75 us
  matrix products: 12.2 us -> 0 us
  local copies, waits for them, and re-layouts: 10.3 us -> 5.06 us
    unnamed x2 -> x0, waiting for transfers between devices: 87.4 us -> none
    unnamed x1 -> x0, blocking collectives: 63.5 us -> none
    pallas_call x0 -> x1, Pallas kernels: none -> 41.5 us  [body(): pl.pallas_call(functools.partial(kernel, n), out_shape=(jax.ShapeDtypeStr...]
    all_to_all x5 -> x0, starting transfers between devices: 24.1 us -> none  [the longest x1 7.41 us: body(): lax.all_to_all(normed, 'ep', split_axis=1, concat_axis=0, tiled=True)]
    all_to_all x5 -> x0, waiting for transfers between devices: 23 us -> none  [the longest x1 6.39 us: body(): lax.all_to_all(outgoing, 'ep', split_axis=0, concat_axis=0, tiled=True)]
    dot_general x14 -> x0, matrix products: 12.2 us -> none  [the longest x1 2.98 us: body(): jnp.dot(hidden, w_down[0], preferred_element_type=jnp.float32)]
    reduce_sum x6 -> x0, other arithmetic: 5.16 us -> none  [the longest x3 4.19 us: rms_scale(): jnp.mean(values * values, axis=-1, keepdims=True) + EPS]
    unnamed x36 -> x4, local copies, waits for them, and re-layouts: 7.66 us -> 5.06 us
  transfers between devices with their start and end apart: 6 -> 0, of which waited for: 5 -> 0; matrix products, arithmetic and copies ran while one was open for 5% -> 0% of each run, Pallas kernels for 0% -> 0%
where the time goes in v1:
time: 49 us; the launch traced here: 48.6 us
  Pallas kernels  41.5 us (85%)
  local copies, waits for them, and re-layouts  5.06 us (10%)
  between operations  1.3 us (3%)
  other arithmetic  0.75 us (2%)
    pallas_call x1, Pallas kernels, body(): pl.pallas_call(functools.partial(kernel, n), out_shape=(jax.ShapeDtypeStr...  41.5 us
    unnamed x4, local copies, waits for them, and re-layouts  5.06 us

profile of v1, /device:TPU:0, one launch (start us, length us, event | category | flops | bytes accessed | tf_op | source)
XLA Modules:
  0.0 48.6 jit_solution(12127241191113294940)
XLA Ops:
  1.3 0.1 fusion
  1.4 0.6 %maximum_maximum_fusion.table_ref = f32[2,32]{1,0:T(2,128)} fusion(f32[1,16]{1,0:T(1,128)S(1)} %get-tuple-element.3, f32[1,16]{1,0:T(1,128)S(1)} %fusion.2, f32[1,16]{1,0:T(1,128)S(1)} %get-tuple-element.4), kind=kLoop, calls=%fused_computation | loop fusion | flops 192 | bytes 448 | tf_op jit(solution)/shard_map/concatenate | solution.py:253
  2.0 1.4 %copy.21.wr_hbm = bf16[128,32]{1,0:T(8,128)(2,1)} copy(bf16[128,32]{0,1:T(8,128)(2,1)} %param.24) | data formatting | bytes 16384 | tf_op args[6]
  3.4 41.5 %shard_map.193 = (bf16[1,2048]{1,0:T(2,128)(2,1)}, bf16[1,512]{1,0:T(2,128)(2,1)}, bf16[1,32]{1,0:T(2,128)(2,1)}) custom-call(bf16[1,2048]{1,0:T(2,128)(2,1)} %tok_ref.1, f32[2,32]{1,0:T(2,128)} %maximum_maximum_fusion.table_ref, f32[1,2048]{1,0:T(1,128)} %bitcast.4, f32[1,512]{1,0:T(1,128)} %bitcast.6, f32[1,2048]{1,0:T(1,128)} %bitcast.5, ...), custom_call_target="tpu_custom_call" | custom-call | tf_op jit(solution)/shard_map/pallas_call | solution.py:267
  45.0 1.3 %copy.26 = bf16[1,2048]{1,0:T(2,128)(2,1)} copy(bf16[1,2048]{1,0:T(2,128)(2,1)} %get-tuple-element.8) | data formatting | bytes 8192
  46.3 1.2 %copy.27 = bf16[1,512]{1,0:T(2,128)(2,1)} copy(bf16[1,512]{1,0:T(2,128)(2,1)} %get-tuple-element.9) | data formatting | bytes 2048
  47.5 1.1 %copy.28 = bf16[1,32]{1,0:T(2,128)(2,1)} copy(bf16[1,32]{1,0:T(2,128)(2,1)} %get-tuple-element.10) | data formatting | bytes 128
  (1 shorter events, 0.0 us)
